TPU v7x, 32 devices: a whole 2x2x4 slice. The times are simulated.
32 devices in a mesh: sp: 8 (over z, y), tp: 4 (over x, core).
Axes of the slice: x: 2, y: 2, z: 4, core: 2. Of those that a mesh axis runs over, the one named last changes fastest.
Arguments:
- grouped_head_inputs: bfloat16 [8192, 2, 1024], P('sp', None, 'tp'), may hold values from -6 to 6
- head_gate_inputs: bfloat16 [8192, 2, 1024], P('sp', None, 'tp'), may hold values from -6 to 6
- unsmoothed_step: float32 [8192, 2, 16], P('sp', None, 'tp'), may hold values from -3.8 to 3.8
- head_decay_rate: float32 [2, 16], P(None, 'tp'), may hold values from 1.2207031e-05 to 0.04761905
- extra_log_decay: float32 [8192, 2, 16], P('sp', None, 'tp'), may hold values from -1.4 to 0
- first_group_keys: bfloat16 [8192, 128], P('sp'), may hold values from -6 to 6
- first_group_queries: bfloat16 [8192, 128], P('sp'), may hold values from -6 to 6
- second_group_keys: bfloat16 [8192, 64], P('sp'), may hold values from -6 to 6
- second_group_queries: bfloat16 [8192, 64], P('sp'), may hold values from -6 to 6
- head_input_filter: float32 [4, 2, 1024], P(None, None, 'tp'), may hold values from -3 to 3
- first_group_filter: float32 [4, 2, 128], replicated, may hold values from -3 to 3
- second_group_filter: float32 [4, 2, 64], replicated, may hold values from -3 to 3
- head_norm_gain: float32 [2, 1024], P(None, 'tp'), may hold values from 0.1 to 1.9
- output_weight: bfloat16 [2, 1024, 2048], P(None, None, 'tp'), may hold values from -0.125 to 0.125
- residual: bfloat16 [8192, 2048], P('sp', 'tp'), may hold values from -37 to 37
- channel_norm_gain: float32 [2048], replicated, may hold values from 0.1 to 1.9
- channel_gate_weight: bfloat16 [2048, 5120], P('sp', 'tp'), may hold values from -0.125 to 0.125
- channel_up_weight: bfloat16 [2048, 5120], P('sp', 'tp'), may hold values from -0.125 to 0.125
- channel_down_weight: bfloat16 [2048, 5120], P('sp', 'tp'), may hold values from -0.078125 to 0.078125
Outputs:
- layer_output: bfloat16 [8192, 2048], P('sp', 'tp')
All inputs are finite; a program needn't handle non-finite values.
Results may differ from a plain program's by a relative error of at most 0.007.
Values may be sent and summed in bfloat16 or wider, within the bound.
A program may use at most 128 MiB of HBM per device.

v0:
```python
import jax
import jax.numpy as jnp
from jax import lax
from jax.sharding import PartitionSpec as P

HEAD = 64
CONV = 4
BLOCK = 128


EPSILON = 1e-06
PRECISE = lax.Precision.HIGHEST


def from_behind(block, axis, distance):
    devices = range(lax.axis_size(axis))
    route = [(i - distance, i) for i in devices if i - distance in devices]
    return lax.ppermute(block, axis, route)


def causal_taps(values, rim_values, taps):
    length = values.shape[0]
    padded = jnp.concatenate([rim_values.astype(jnp.float32), values.astype(jnp.float32)], axis=0)
    running = jnp.zeros(values.shape, jnp.float32)
    for offset in range(CONV):
        running = running + taps[offset] * padded[offset : offset + length]
    return jax.nn.silu(running)


def block_pass(current, value_rows, log_rows, key_rows, query_rows):
    cumulative = jnp.cumsum(log_rows, axis=0)
    length = value_rows.shape[0]
    causal = jnp.arange(length)[:, None] >= jnp.arange(length)[None, :]
    scores = jnp.dot(query_rows, key_rows.T, precision=PRECISE)
    span_logs = jnp.where(
        causal[:, :, None], cumulative[:, None, :] - cumulative[None, :, :], -jnp.inf
    )
    weights = jnp.exp(span_logs) * scores[:, :, None]
    inside = jnp.einsum("lsh,shp->lhp", weights, value_rows, precision=PRECISE)
    carried = (
        jnp.einsum("ls,hps->lhp", query_rows, current, precision=PRECISE)
        * jnp.exp(cumulative)[:, :, None]
    )
    to_end = jnp.exp(cumulative[-1][None, :] - cumulative)
    update = jnp.einsum("lhp,ls->hps", value_rows * to_end[:, :, None], key_rows, precision=PRECISE)
    new_state = current * jnp.exp(cumulative[-1])[:, None, None] + update
    return (new_state, inside + carried)


def scan_group(value_rows, log_rows, key_rows, query_rows):
    length, head_count, head_width = value_rows.shape
    block_count = length // BLOCK
    initial = jnp.zeros((head_count, head_width, key_rows.shape[1]), jnp.float32)
    blocks = (
        value_rows.reshape(block_count, BLOCK, head_count, head_width),
        log_rows.reshape(block_count, BLOCK, head_count),
        key_rows.reshape(block_count, BLOCK, -1),
        query_rows.reshape(block_count, BLOCK, -1),
    )

    def advance(current, pieces):
        return block_pass(current, pieces[0], pieces[1], pieces[2], pieces[3])

    final_state, outputs = lax.scan(advance, initial, blocks)
    return (final_state, outputs.reshape(length, head_count, head_width))


def shards(
    grouped_head_inputs,
    head_gate_inputs,
    unsmoothed_step,
    head_decay_rate,
    extra_log_decay,
    first_group_keys,
    first_group_queries,
    second_group_keys,
    second_group_queries,
    head_input_filter,
    first_group_filter,
    second_group_filter,
    head_norm_gain,
    output_weight,
    residual,
    channel_norm_gain,
    channel_gate_weight,
    channel_up_weight,
    channel_down_weight,
):
    rim_rows = CONV - 1
    rims = from_behind(
        (
            grouped_head_inputs[-rim_rows:],
            first_group_keys[-rim_rows:],
            first_group_queries[-rim_rows:],
            second_group_keys[-rim_rows:],
            second_group_queries[-rim_rows:],
        ),
        "sp",
        1,
    )
    conv_heads = causal_taps(grouped_head_inputs, rims[0], head_input_filter)
    keys_one = causal_taps(first_group_keys, rims[1], first_group_filter[:, 0])
    queries_one = causal_taps(first_group_queries, rims[2], first_group_filter[:, 1])
    keys_two = causal_taps(second_group_keys, rims[3], second_group_filter[:, 0])
    queries_two = causal_taps(second_group_queries, rims[4], second_group_filter[:, 1])
    length = grouped_head_inputs.shape[0]
    local_heads = head_decay_rate.shape[1]
    head_step_size = jax.nn.softplus(unsmoothed_step)
    decay_logarithm = extra_log_decay - head_step_size * head_decay_rate[None]
    values = conv_heads.reshape(length, 2, local_heads, HEAD) * head_step_size[:, :, :, None]
    state_one, local_one = scan_group(values[:, 0], decay_logarithm[:, 0], keys_one, queries_one)
    state_two, local_two = scan_group(values[:, 1], decay_logarithm[:, 1], keys_two, queries_two)
    running = jnp.cumsum(decay_logarithm, axis=0)
    device_log = running[-1]
    gathered = (
        lax.all_gather(device_log[None].astype(jnp.bfloat16), "sp", axis=0, tiled=True).astype(
            jnp.float32
        ),
        lax.all_gather(state_one[None].astype(jnp.bfloat16), "sp", axis=0, tiled=True).astype(
            jnp.float32
        ),
        lax.all_gather(state_two[None].astype(jnp.bfloat16), "sp", axis=0, tiled=True).astype(
            jnp.float32
        ),
    )
    logs_all = gathered[0]
    inclusive = jnp.cumsum(logs_all, axis=0)
    exclusive = inclusive - logs_all
    position = lax.axis_index("sp")
    device_ids = jnp.arange(lax.axis_size("sp"), dtype=jnp.int32)
    mine = jnp.sum(jnp.where((device_ids == position)[:, None, None], exclusive, 0.0), axis=0)
    earlier = (device_ids < position)[:, None, None]
    factors = jnp.exp(jnp.where(earlier, mine[None] - inclusive, -jnp.inf))
    enter_one = jnp.einsum("kh,khps->hps", factors[:, 0], gathered[1], precision=PRECISE)
    enter_two = jnp.einsum("kh,khps->hps", factors[:, 1], gathered[2], precision=PRECISE)
    carried_one = (
        jnp.einsum("ls,hps->lhp", queries_one, enter_one, precision=PRECISE)
        * jnp.exp(running[:, 0])[:, :, None]
    )
    carried_two = (
        jnp.einsum("ls,hps->lhp", queries_two, enter_two, precision=PRECISE)
        * jnp.exp(running[:, 1])[:, :, None]
    )
    mixer = jnp.stack([local_one + carried_one, local_two + carried_two], axis=1)
    gated = mixer * jax.nn.silu(head_gate_inputs.astype(jnp.float32)).reshape(
        length, 2, local_heads, HEAD
    )
    scaled = gated * lax.rsqrt(jnp.mean(gated * gated, axis=3, keepdims=True) + EPSILON)
    mixed = (scaled.reshape(length, 2, -1) * head_norm_gain[None]).astype(jnp.bfloat16)
    projected = jnp.einsum(
        "tgc,gcd->td",
        lax.all_gather(mixed, "tp", axis=2, tiled=True),
        output_weight,
        preferred_element_type=jnp.float32,
    )
    stream = (residual.astype(jnp.float32) + projected).astype(jnp.bfloat16)
    full_rows = lax.all_gather(stream, "tp", axis=1, tiled=True).astype(jnp.float32)
    normed = (
        full_rows
        * lax.rsqrt(jnp.mean(full_rows * full_rows, axis=1, keepdims=True) + EPSILON)
        * channel_norm_gain[None]
    ).astype(jnp.bfloat16)
    contract_last = (((1,), (1,)), ((), ()))
    gate_full, up_full = (
        lax.all_gather(channel_gate_weight, "sp", axis=0, tiled=True),
        lax.all_gather(channel_up_weight, "sp", axis=0, tiled=True),
    )
    gate = jnp.dot(normed, gate_full, preferred_element_type=jnp.float32)
    upward = jnp.dot(normed, up_full, preferred_element_type=jnp.float32)
    hidden = (jax.nn.silu(gate) * upward).astype(jnp.bfloat16)
    partial_value = lax.dot_general(
        hidden,
        lax.all_gather(channel_down_weight, "sp", axis=0, tiled=True),
        contract_last,
        preferred_element_type=jnp.float32,
    )
    summed = lax.psum_scatter(
        partial_value.astype(jnp.bfloat16), "tp", scatter_dimension=1, tiled=True
    ).astype(jnp.float32)
    return (stream.astype(jnp.float32) + 0.5 * summed).astype(jnp.bfloat16)


def solution(mesh):
    return jax.shard_map(
        shards,
        mesh=mesh,
        in_specs=(
            P("sp", None, "tp"),
            P("sp", None, "tp"),
            P("sp", None, "tp"),
            P(None, "tp"),
            P("sp", None, "tp"),
            P("sp", None),
            P("sp", None),
            P("sp", None),
            P("sp", None),
            P(None, None, "tp"),
            P(),
            P(),
            P(None, "tp"),
            P(None, None, "tp"),
            P("sp", "tp"),
            P(),
            P("sp", "tp"),
            P("sp", "tp"),
            P("sp", "tp"),
        ),
        out_specs=P("sp", "tp"),
        check_vma=False,
    )
```

profile of v0, /device:TPU:0, one launch (start us, length us, event | category | flops | bytes accessed | tf_op | source)
XLA Modules:
  0.0 757.3 jit_solution(4832280834423593863)
XLA Ops:
  7.9 5.4 collective-permute-start.2
  54.3 17.3 %all_gather.24 = bf16[8,2,4]{2,1,0:T(2,128)(2,1)S(1)} all-gather(bf16[1,2,4]{2,1,0:T(2,128)(2,1)} %slice.463), channel_id=1, replica_groups=mesh['sp'=8,'tp'=4] {'sp'}, dimensions={0}, use_global_device_ids=true | all-gather | bytes 144 | tf_op jit(solution)/shard_map/all_gather | solution.py:116
  99.1 82.8 %while.26 = (s32[]{:T(128)}, f32[4,64,128]{2,1,0:T(8,128)S(1)}, f32[8,128,4,64]{1,0,3,2:T(8,128)}, f32[8,128,4]{2,1,0:T(8,128)}, f32[8,128,4,64]{1,0,3,2:T(8,128...) while((s32[]{:T(128)}, f32[4,64,128]{2,1,0:T(8,128)S(1)}, ...), condition=%wide.region_2.3_spmd.clone, body=%wide.region_0.2_spmd.clone.sunk | while | flops 176668672 | bytes 2033380 | solution.py:64
  103.8 4.4 dynamic_update_slice.11
  114.1 4.4 dynamic_update_slice.11
  124.5 4.4 dynamic_update_slice.11
  134.8 4.4 dynamic_update_slice.11
  145.2 4.4 dynamic_update_slice.11
  155.5 4.4 dynamic_update_slice.11
  165.9 4.4 dynamic_update_slice.11
  176.2 4.4 dynamic_update_slice.11
  182.0 33.7 %all-gather = bf16[32,64,128]{2,1,0:T(8,128)(2,1)} all-gather(bf16[4,64,128]{2,1,0:T(8,128)(2,1)S(1)} %convert_element_type.89), channel_id=2, replica_groups=mesh['sp'=8,'tp'=4] {'sp'}, dimensions={0}, use_global_device_ids=true | all-gather | bytes 589824 | tf_op jit(solution)/shard_map/all_gather | solution.py:119
  221.4 78.1 %while.27 = (s32[]{:T(128)}, f32[4,64,64]{2,1,0:T(8,128)S(1)}, f32[8,128,4,64]{1,0,3,2:T(8,128)}, f32[8,128,4]{2,1,0:T(8,128)}, f32[8,128,4,64]{1,0,3,2:T(8,128)...) while((s32[]{:T(128)}, f32[4,64,64]{2,1,0:T(8,128)S(1)}, ...), condition=%wide.region_9.10_spmd.clone, body=%wide.region_7.9_spmd.clone.sunk | while | flops 113688576 | bytes 1835236 | solution.py:64
  245.8 4.4 dynamic_update_slice.12
  299.5 31.6 %all-gather.1 = bf16[32,64,64]{2,1,0:T(8,128)(2,1)S(1)} all-gather(bf16[4,64,64]{2,1,0:T(8,128)(2,1)S(1)} %convert_element_type.95), channel_id=3, replica_groups=mesh['sp'=8,'tp'=4] {'sp'}, dimensions={0}, use_global_device_ids=true | all-gather | bytes 294912 | tf_op jit(solution)/shard_map/all_gather | solution.py:122
  351.9 32.7 %all-gather.8.cloned.1.call-done = bf16[1024,2,1024]{2,0,1:T(8,128)(2,1)} async-done(((bf16[1024,2,256]{2,0,1:T(8,128)(2,1)}), bf16[1024,2,1024]{2,0,1:T(8,128)(2,1)}) %all-gather.8.cloned.1.call-update) | async-done | bytes 4194320 | tf_op jit(solution)/shard_map/all_gather | solution.py:152
  384.6 5.8 fusion.69
  392.6 32.4 %all-gather.10.cloned.1.call-done = bf16[1024,2048]{1,0:T(8,128)(2,1)} async-done(((bf16[1024,512]{1,0:T(8,128)(2,1)}), bf16[1024,2048]{1,0:T(8,128)(2,1)}) %all-gather.10.cloned.1.call-update) | async-done | bytes 4194320 | tf_op jit(solution)/shard_map/all_gather | solution.py:157
  428.1 85.0 %all-gather.12.cloned.1.call-done = bf16[2048,1280]{1,0:T(8,128)(2,1)} async-done(((bf16[256,1280]{1,0:T(8,128)(2,1)}), bf16[2048,1280]{1,0:T(8,128)(2,1)}) %all-gather.12.cloned.1.call-update) | async-done | bytes 5242896 | tf_op jit(solution)/shard_map/all_gather | solution.py:165
  513.1 10.7 %fusion.73 = f32[1024,1280]{1,0:T(8,128)} fusion(bf16[2048,1280]{1,0:T(8,128)(2,1)} %all-gather.12.cloned.1.call-done, bf16[1024,2048]{1,0:T(8,128)(2,1)} %all-gather.10.cloned.1.call-done, f32[2048]{0:T(1024)S(1)} %copy-done.24, f32[1024]{0:T(1024)S(1)} %add_rsqrt_fusion.1), kind=kOutput, calls=%fused_computation.106 | convolution fusion | flops 5377097728 | bytes 14692352 | tf_op jit(solution)/shard_map/dot_general | solution.py:168
  523.8 75.4 %all-gather.14.cloned.1.call-done = bf16[2048,1280]{1,0:T(8,128)(2,1)} async-done(((bf16[256,1280]{1,0:T(8,128)(2,1)}), bf16[2048,1280]{1,0:T(8,128)(2,1)}) %all-gather.14.cloned.1.call-update) | async-done | bytes 5242896 | tf_op jit(solution)/shard_map/all_gather | solution.py:166
  599.3 86.1 %all-gather.16.cloned.1.call-done = bf16[2048,1280]{1,0:T(8,128)(2,1)} async-done(((bf16[256,1280]{1,0:T(8,128)(2,1)}), bf16[2048,1280]{1,0:T(8,128)(2,1)}) %all-gather.16.cloned.1.call-update) | async-done | bytes 5242896 | tf_op jit(solution)/shard_map/all_gather | solution.py:173
  685.4 19.8 %convolution_convert_fusion = bf16[1024,2048]{1,0:T(8,128)(2,1)} fusion(bf16[2048,1280]{1,0:T(8,128)(2,1)} %all-gather.16.cloned.1.call-done, f32[1024,1280]{1,0:T(8,128)} %fusion.73, bf16[2048,1280]{1,0:T(8,128)(2,1)} %all-gather.14.cloned.1.call-done, bf16[1024,2048]{1,0:T(8,128)(2,1)} %all-gather.10.cloned.1.call-done, f32[2048]{0:T(1024)S(1)} %copy-done.24, ...), kind=kOutput, calls=%fused_computation.74 | convolution fusion | flops 10755768320 | bytes 24129536 | tf_op jit(solution)/shard_map/dot_general | solution.py:171
  705.2 42.7 %reduce-scatter.2.cloned.1.call-done = bf16[1024,512]{1,0:T(8,128)(2,1)} async-done(((bf16[1024,2048]{1,0:T(8,128)(2,1)}), bf16[1024,512]{1,0:T(8,128)(2,1)}) %reduce-scatter.2.cloned.1.call-update) | async-done | bytes 1048592 | tf_op jit(solution)/shard_map/reduce_scatter | solution.py:177
  (386 shorter events, 223.8 us)
Async XLA Ops:
  6.5 378.1 %copy-start = (bf16[2,1024,512]{2,1,0:T(8,128)(2,1)S(1)}, bf16[2,1024,512]{2,1,0:T(8,128)(2,1)}, u32[]{:S(2)}) copy-start(bf16[2,1024,512]{2,1,0:T(8,128)(2,1)} %param.36) | copy-start | bytes 6291460
  6.5 29.5 %copy-start.15 = (bf16[1024,2,256]{2,1,0:T(2,128)(2,1)S(1)}, bf16[1024,2,256]{2,1,0:T(2,128)(2,1)}, u32[]{:S(2)}) copy-start(bf16[1024,2,256]{2,1,0:T(2,128)(2,1)} %param.23) | copy-start | bytes 3145732
  6.5 378.1 %all-gather.8.cloned.1.call-start = ((), (), s32[]{:S(2)}) async-start(), calls=%async_computation.1 | async-start | bytes 5242880 | tf_op jit(solution)/shard_map/all_gather | solution.py:152
  7.9 77.4 %collective-permute-start.2 = (bf16[3,128]{1,0:T(4,128)(2,1)}, bf16[3,128]{1,0:T(4,128)(2,1)}, u32[]{:S(2)}, u32[]{:S(2)}) collective-permute-start(bf16[3,128]{1,0:T(4,128)(2,1)} %slice.217), channel_id=1, source_target_pairs={{0,4},{4,8},{8,12},{12,16},{16,20},{20,24},{24,28},{1,5},{5,9},{9,... | collective-permute-start | bytes 2312 | tf_op jit(solution)/shard_map/ppermute | solution.py:18
  14.6 71.7 %collective-permute-start.1 = (bf16[3,128]{1,0:T(4,128)(2,1)}, bf16[3,128]{1,0:T(4,128)(2,1)}, u32[]{:S(2)}, u32[]{:S(2)}) collective-permute-start(bf16[3,128]{1,0:T(4,128)(2,1)} %slice.209), channel_id=1, source_target_pairs={{0,4},{4,8},{8,12},{12,16},{16,20},{20,24},{24,28},{1,5},{5,9},{9,... | collective-permute-start | bytes 2312 | tf_op jit(solution)/shard_map/ppermute | solution.py:18
  19.3 68.8 %collective-permute-start = (bf16[3,2,256]{2,0,1:T(4,128)(2,1)}, bf16[3,2,256]{2,0,1:T(4,128)(2,1)}, u32[]{:S(2)}, u32[]{:S(2)}) collective-permute-start(bf16[3,2,256]{2,0,1:T(4,128)(2,1)} %copy.130), channel_id=1, source_target_pairs={{0,4},{4,8},{8,12},{12,16},{16,20},{20,24},{24,28},{1,5},{5,9},{9,... | collective-permute-start | bytes 9224 | tf_op jit(solution)/shard_map/ppermute | solution.py:18
  24.2 57.1 %collective-permute-start.4 = (bf16[3,64]{0,1:T(8,128)(2,1)}, bf16[3,64]{0,1:T(8,128)(2,1)}, u32[]{:S(2)}, u32[]{:S(2)}) collective-permute-start(bf16[3,64]{0,1:T(8,128)(2,1)} %slice.240), channel_id=1, source_target_pairs={{0,4},{4,8},{8,12},{12,16},{16,20},{20,24},{24,28},{1,5},{5,9},{9,... | collective-permute-start | bytes 1160 | tf_op jit(solution)/shard_map/ppermute | solution.py:18
  29.0 53.4 %collective-permute-start.3 = (bf16[3,64]{0,1:T(8,128)(2,1)}, bf16[3,64]{0,1:T(8,128)(2,1)}, u32[]{:S(2)}, u32[]{:S(2)}) collective-permute-start(bf16[3,64]{0,1:T(8,128)(2,1)} %slice.232), channel_id=1, source_target_pairs={{0,4},{4,8},{8,12},{12,16},{16,20},{20,24},{24,28},{1,5},{5,9},{9,... | collective-permute-start | bytes 1160 | tf_op jit(solution)/shard_map/ppermute | solution.py:18
  37.5 11.2 %copy-start.18 = (bf16[1024,64]{0,1:T(8,128)(2,1)S(1)}, bf16[1024,64]{0,1:T(8,128)(2,1)}, u32[]{:S(2)}) copy-start(bf16[1024,64]{0,1:T(8,128)(2,1)} %param.31) | copy-start | bytes 393220
  43.4 30.5 %copy-start.7 = (bf16[1024,2,256]{2,1,0:T(2,128)(2,1)S(1)}, bf16[1024,2,256]{2,1,0:T(2,128)(2,1)}, u32[]{:S(2)}) copy-start(bf16[1024,2,256]{2,1,0:T(2,128)(2,1)} %param.24) | copy-start | bytes 3145732
  78.2 5.2 copy-start.16
  81.2 4.7 copy-start.14
  81.2 5.7 copy-start.13
  82.1 6.7 copy-start.4
  181.9 38.5 %copy-start.5 = (f32[8,128,128]{2,1,0:T(8,128)}, f32[8,128,128]{2,1,0:T(8,128)S(1)}, u32[]{:S(2)}) copy-start(f32[8,128,128]{2,1,0:T(8,128)S(1)} %get-tuple-element.393) | copy-start | bytes 1572868
  299.5 34.0 %copy-start.12 = (bf16[32,64,128]{2,1,0:T(8,128)(2,1)S(1)}, bf16[32,64,128]{2,1,0:T(8,128)(2,1)}, u32[]{:S(2)}) copy-start(bf16[32,64,128]{2,1,0:T(8,128)(2,1)} %all-gather) | copy-start | bytes 1572868
  351.8 73.2 %all-gather.10.cloned.1.call-start = ((), (), s32[]{:S(2)}) async-start(), calls=%async_computation.2 | async-start | bytes 5242880 | tf_op jit(solution)/shard_map/all_gather | solution.py:157
  390.4 122.7 %all-gather.12.cloned.1.call-start = ((), (), s32[]{:S(2)}) async-start(), calls=%async_computation.3 | async-start | bytes 5898240 | tf_op jit(solution)/shard_map/all_gather | solution.py:165
  391.1 208.1 %all-gather.14.cloned.1.call-start = ((), (), s32[]{:S(2)}) async-start(), calls=%async_computation.4 | async-start | bytes 5898240 | tf_op jit(solution)/shard_map/all_gather | solution.py:166
  391.7 293.7 %all-gather.16.cloned.1.call-start = ((), (), s32[]{:S(2)}) async-start(), calls=%async_computation.5 | async-start | bytes 5898240 | tf_op jit(solution)/shard_map/all_gather | solution.py:173
  392.3 120.8 %copy-start.24 = (f32[2048]{0:T(1024)S(1)}, f32[2048]{0:T(1024)}, u32[]{:S(2)}) copy-start(f32[2048]{0:T(1024)} %param.38) | copy-start | bytes 24580
  392.3 355.6 %reduce-scatter.2.cloned.1.call-start = ((), (), s32[]{:S(2)}) async-start(), calls=%async_computation.6 | async-start | bytes 5242880 | tf_op jit(solution)/shard_map/reduce_scatter | solution.py:177
  705.2 42.8 %copy-start.6 = (bf16[1024,512]{1,0:T(8,128)(2,1)S(1)}, bf16[1024,512]{1,0:T(8,128)(2,1)}, u32[]{:S(2)}) copy-start(bf16[1024,512]{1,0:T(8,128)(2,1)} %fusion.69) | copy-start | bytes 3145732
  705.2 45.2 %copy-start.1 = (bf16[2,1024,512]{2,1,0:T(8,128)(2,1)S(1)}, bf16[2,1024,512]{2,1,0:T(8,128)(2,1)}, u32[]{:S(2)}) copy-start(bf16[2,1024,512]{2,1,0:T(8,128)(2,1)} %param.36) | copy-start | bytes 6291460
  (12 other events, 39.2 us)
Sparse Core Ops, SparseCore 0:
  352.0 32.5 all-gather.7
  390.5 34.4 all-gather.9
  427.2 85.8 all-gather.11
  515.2 84.0 all-gather.13
  601.3 84.0 all-gather.15
  705.3 42.5 reduce-scatter.1
where the time goes:
time: 762 us; the launch traced here: 757 us
  waiting for transfers between devices  356 us (47%)
  local copies, waits for them, and re-layouts  167 us (22%)
  blocking collectives  82.6 us (11%)
  matrix products  79.8 us (10%)
  other arithmetic  36.8 us (5%)
  starting transfers between devices  19.6 us (3%)
  between operations  13.8 us (2%)
    all_gather x1, waiting for transfers between devices, shards(): lax.all_gather(channel_down_weight, 'sp', axis=0, tiled=True)  86.1 us
    all_gather x1, waiting for transfers between devices, shards(): lax.all_gather(channel_gate_weight, 'sp', axis=0, tiled=True)  85 us
    all_gather x1, waiting for transfers between devices, shards(): lax.all_gather(channel_up_weight, 'sp', axis=0, tiled=True)  75.4 us
    dynamic_update_slice x16, local copies, waits for them, and re-layouts, scan_group(): final_state, outputs = lax.scan(advance, initial, blocks)  71.1 us
    reduce_scatter x1, waiting for transfers between devices, shards(): lax.psum_scatter(partial_value.astype(jnp.bfloat16), 'tp', scatter_dimens...  42.7 us
    all_gather x1, blocking collectives, shards(): lax.all_gather(state_one[None].astype(jnp.bfloat16), 'sp', axis=0, tiled=...  33.7 us
    all_gather x1, waiting for transfers between devices, shards(): lax.all_gather(mixed, 'tp', axis=2, tiled=True)  32.7 us
    all_gather x1, waiting for transfers between devices, shards(): lax.all_gather(stream, 'tp', axis=1, tiled=True).astype(jnp.float32)  32.4 us
  transfers between devices with their start and end apart: 11, of which 6 were waited for; matrix products, arithmetic and copies ran while one was open for 8% of the time, Pallas kernels for 0%

commit v1 on v0

v1 whole, which is shorter than its diff:
```python
import functools

import jax
import jax.numpy as jnp
from jax import lax
from jax.experimental import pallas as pl
from jax.experimental.pallas import tpu as pltpu
from jax.sharding import PartitionSpec as P

HEAD = 64
CONV = 4
BLOCK = 128
RIM = 16
EPSILON = 1e-06
MESH = pl.DeviceIdType.MESH


def rows_of(b):
    return pl.ds(pl.multiple_of(b * BLOCK, BLOCK), BLOCK)


def spread(columns, first, count):
    parts = [
        jnp.broadcast_to(columns[:, h : h + 1], (columns.shape[0], HEAD))
        for h in range(first, first + count)
    ]
    return jnp.concatenate(parts, axis=1)


def sigmoid(x):
    return 1.0 / (1.0 + jnp.exp(-x))


def front_kernel(
    n, tp, heads, s1, s2,
    x_ref, gate_ref, log_ref, step_ref, taps_ref, hgain_ref, wout_ref, res_ref, cgain_ref,
    normed_ref, own_ref,
    xs, rim, vals, kq, cums, st, stsend, strecv, mix, stream,
    rim_sems, st_send, st_recv, m_send, m_fwd, m_recv, r_send, r_fwd, r_recv,
):
    me = lax.axis_index("sp")
    t = lax.axis_index("tp")
    half = heads * HEAD
    wide = 2 * half
    nb = x_ref.shape[0] // BLOCK
    nx = tp // 2
    core = lax.rem(t, 2)
    my_x = t // 2
    partner = my_x * 2 + (1 - core)

    rim_copy = pltpu.make_async_remote_copy(
        src_ref=x_ref.at[pl.ds(x_ref.shape[0] - RIM, RIM)],
        dst_ref=rim,
        send_sem=rim_sems.at[0],
        recv_sem=rim_sems.at[1],
        device_id={"sp": lax.rem(me + 1, n)},
        device_id_type=MESH,
    )

    @pl.when(me < n - 1)
    def _():
        rim_copy.start()

    @pl.when(me > 0)
    def _():
        rim_copy.wait_recv()
        xs[...] = rim[...].astype(jnp.float32)[RIM - 8 :]

    @pl.when(me == 0)
    def _():
        xs[...] = jnp.zeros_like(xs)

    st[...] = jnp.zeros_like(st)
    row_i = lax.broadcasted_iota(jnp.int32, (BLOCK, BLOCK), 0)
    col_i = lax.broadcasted_iota(jnp.int32, (BLOCK, BLOCK), 1)
    causal = row_i >= col_i
    tri = jnp.where(causal, 1.0, 0.0).astype(jnp.float32)

    def state_update(b, cum):
        last = cum[BLOCK - 1 : BLOCK]
        to_end = jnp.exp(last - cum)
        decay = jnp.exp(last)
        r = rows_of(b)
        for g in range(2):
            k0, size = (wide, s1) if g == 0 else (wide + 2 * s1, s2)
            base = 0 if g == 0 else s1
            keys = kq[r, k0 - wide : k0 - wide + size]
            v = vals[r, g * half : (g + 1) * half].astype(jnp.float32)
            v = (v * spread(to_end, g * heads, heads)).astype(jnp.bfloat16)
            add = lax.dot_general(
                keys, v, (((0,), (0,)), ((), ())), preferred_element_type=jnp.float32
            )
            st[base : base + size] = (
                st[base : base + size] * spread(decay, g * heads, heads) + add
            )

    def first_pass(b, total):
        r = rows_of(b)
        current = x_ref[r].astype(jnp.float32)
        taps = taps_ref[...]
        extended = jnp.concatenate([xs[...], current], axis=0)
        acc = taps[CONV - 1 : CONV] * current
        for k in range(CONV - 1):
            acc = acc + taps[k : k + 1] * pltpu.roll(extended, CONV - 1 - k, 0)[8:]
        xs[...] = current[BLOCK - 8 :]
        acc = acc * sigmoid(acc)
        vals[r] = (acc[:, :wide] * spread(step_ref[r], 0, 2 * heads)).astype(jnp.bfloat16)
        kq[r] = acc[:, wide:].astype(jnp.bfloat16)
        cum = jnp.dot(
            tri, log_ref[r], precision=lax.Precision.HIGHEST, preferred_element_type=jnp.float32
        )
        cums[r] = cum
        state_update(b, cum)
        return total + cum[BLOCK - 1 : BLOCK]

    total = lax.fori_loop(0, nb, first_pass, jnp.zeros((1, log_ref.shape[1]), jnp.float32))

    states = s1 + s2
    stsend[0:states] = st[...].astype(jnp.bfloat16)
    which = lax.broadcasted_iota(jnp.int32, (RIM, half), 0)
    extra = jnp.zeros((RIM, half), jnp.float32)
    for g in range(2):
        logs = spread(total, g * heads, heads)
        high = logs.astype(jnp.bfloat16).astype(jnp.float32)
        low = logs - high
        extra = jnp.where(which == g, high, extra)
        extra = jnp.where(which == 2 + g, low, extra)
    stsend[states : states + RIM] = extra.astype(jnp.bfloat16)

    def state_copy(to, source):
        return pltpu.make_async_remote_copy(
            src_ref=stsend,
            dst_ref=strecv.at[source],
            send_sem=st_send.at[to],
            recv_sem=st_recv.at[source],
            device_id={"sp": to},
            device_id_type=MESH,
        )

    def send_state(to, carry):
        state_copy(to, me).start()
        return carry

    lax.fori_loop(me + 1, n, send_state, 0)
    st[...] = jnp.zeros_like(st)

    def take_state(source, carry):
        state_copy(n - 1, source).wait_recv()
        got = strecv[source].astype(jnp.float32)
        for g in range(2):
            base, size = (0, s1) if g == 0 else (s1, s2)
            logs = got[states + g : states + g + 1] + got[states + 2 + g : states + 3 + g]
            st[base : base + size] = st[base : base + size] * jnp.exp(logs) + got[base : base + size]
        return carry

    lax.fori_loop(0, me, take_state, 0)

    def share(buf, source, b, to, send, recv):
        piece = buf.at[source, rows_of(b)]
        return pltpu.make_async_remote_copy(
            src_ref=piece,
            dst_ref=piece,
            send_sem=send,
            recv_sem=recv.at[source, b],
            device_id={"tp": to},
            device_id_type=MESH,
        )

    def across(d):
        return lax.rem(my_x + d, nx) * 2

    def send_own(buf, b, send, recv):
        for d in range(1, nx):
            to = across(d) + core
            share(buf, t, b, to, send.at[d, b], recv).start()
        share(buf, t, b, partner, send.at[0, b], recv).start()

    def forward(buf, b, fwd, recv):
        for d in range(1, nx):
            source = across(d) + core
            move = share(buf, source, b, partner, fwd.at[d, b], recv)
            move.wait_recv()
            move.start()

    def wait_rest(buf, b, send, recv):
        share(buf, partner, b, partner, send.at[0, b], recv).wait_recv()
        for d in range(1, nx):
            source = across(d) + (1 - core)
            share(buf, source, b, partner, send.at[0, b], recv).wait_recv()

    def second_pass(b):
        r = rows_of(b)
        cum = cums[r]
        cum_t = cum.T
        grown = jnp.exp(cum)
        for g in range(2):
            off, size = (0, s1) if g == 0 else (2 * s1, s2)
            base = 0 if g == 0 else s1
            keys = kq[r, off : off + size]
            queries = kq[r, off + size : off + 2 * size]
            scores = lax.dot_general(
                queries, keys, (((1,), (1,)), ((), ())), preferred_element_type=jnp.float32
            )
            carried = jnp.dot(
                queries,
                st[base : base + size].astype(jnp.bfloat16),
                preferred_element_type=jnp.float32,
            )
            carried = carried * spread(grown, g * heads, heads)
            v = vals[r, g * half : (g + 1) * half]
            outs = []
            for h in range(heads):
                c = g * heads + h
                span = jnp.where(causal, cum[:, c : c + 1] - cum_t[c : c + 1, :], -jnp.inf)
                w = (jnp.exp(span) * scores).astype(jnp.bfloat16)
                lanes = slice(h * HEAD, (h + 1) * HEAD)
                y = jnp.dot(w, v[:, lanes], preferred_element_type=jnp.float32)
                y = y + carried[:, lanes]
                z = gate_ref[r, g * half + h * HEAD : g * half + (h + 1) * HEAD].astype(jnp.float32)
                y = y * (z * sigmoid(z))
                y = y * lax.rsqrt(jnp.mean(y * y, axis=1, keepdims=True) + EPSILON)
                outs.append(y)
            out = jnp.concatenate(outs, axis=1) * hgain_ref[:, g * half : (g + 1) * half]
            mix[t, r, g * half : (g + 1) * half] = out.astype(jnp.bfloat16)
        state_update(b, cum)
        send_own(mix, b, m_send, m_recv)

    def project(b):
        r = rows_of(b)
        wait_rest(mix, b, m_send, m_recv)
        acc = res_ref[r].astype(jnp.float32)
        for source in range(tp):
            acc = acc + jnp.dot(
                mix[source, r], wout_ref[source], preferred_element_type=jnp.float32
            )
        value = acc.astype(jnp.bfloat16)
        own_ref[r] = value
        stream[t, r] = value
        send_own(stream, b, r_send, r_recv)

    def normalise(b):
        r = rows_of(b)
        wait_rest(stream, b, r_send, r_recv)
        cols = own_ref.shape[1]
        parts = [stream[source, r].astype(jnp.float32) for source in range(tp)]
        square = sum(jnp.sum(p * p, axis=1, keepdims=True) for p in parts)
        scale = lax.rsqrt(square / (tp * cols) + EPSILON)
        for source in range(tp):
            lanes = slice(source * cols, (source + 1) * cols)
            normed_ref[r, lanes] = (parts[source] * scale * cgain_ref[:, lanes]).astype(
                jnp.bfloat16
            )

    def stage(b, carry):
        @pl.when(b < nb)
        def _():
            second_pass(b)

        @pl.when((b >= 1) & (b < nb + 1))
        def _():
            forward(mix, b - 1, m_fwd, m_recv)

        @pl.when((b >= 2) & (b < nb + 2))
        def _():
            project(b - 2)

        @pl.when((b >= 3) & (b < nb + 3))
        def _():
            forward(stream, b - 3, r_fwd, r_recv)

        @pl.when(b >= 4)
        def _():
            normalise(b - 4)

        return carry

    lax.fori_loop(0, nb + 4, stage, 0)

    @pl.when(me < n - 1)
    def _():
        rim_copy.wait_send()

    def end_state(to, carry):
        state_copy(to, me).wait_send()
        return carry

    lax.fori_loop(me + 1, n, end_state, 0)

    def end_shares(b, carry):
        for buf, send, fwd, recv in (
            (mix, m_send, m_fwd, m_recv),
            (stream, r_send, r_fwd, r_recv),
        ):
            for d in range(nx):
                share(buf, t, b, partner, send.at[d, b], recv).wait_send()
            for d in range(1, nx):
                share(buf, t, b, partner, fwd.at[d, b], recv).wait_send()
        return carry

    lax.fori_loop(0, nb, end_shares, 0)


def front(x, gate, logs, step, taps, hgain, wout, residual, cgain, heads, s1, s2):
    n, tp = lax.axis_size("sp"), lax.axis_size("tp")
    tokens, lanes = x.shape
    half = heads * HEAD
    cols = residual.shape[1]
    nb = tokens // BLOCK
    vmem = pl.BlockSpec(memory_space=pltpu.VMEM)
    dma = pltpu.SemaphoreType.DMA
    return pl.pallas_call(
        functools.partial(front_kernel, n, tp, heads, s1, s2),
        out_shape=(
            jax.ShapeDtypeStruct((tokens, tp * cols), jnp.bfloat16),
            jax.ShapeDtypeStruct((tokens, cols), jnp.bfloat16),
        ),
        in_specs=[vmem] * 9,
        out_specs=(vmem, vmem),
        scratch_shapes=[
            pltpu.VMEM((8, lanes), jnp.float32),
            pltpu.VMEM((RIM, lanes), jnp.bfloat16),
            pltpu.VMEM((tokens, 2 * half), jnp.bfloat16),
            pltpu.VMEM((tokens, 2 * (s1 + s2)), jnp.bfloat16),
            pltpu.VMEM((tokens, logs.shape[1]), jnp.float32),
            pltpu.VMEM((s1 + s2, half), jnp.float32),
            pltpu.VMEM((s1 + s2 + RIM, half), jnp.bfloat16),
            pltpu.VMEM((n, s1 + s2 + RIM, half), jnp.bfloat16),
            pltpu.VMEM((tp, tokens, 2 * half), jnp.bfloat16),
            pltpu.VMEM((tp, tokens, cols), jnp.bfloat16),
            dma((2,)),
            dma((n,)),
            dma((n,)),
            dma((tp, nb)),
            dma((tp, nb)),
            dma((tp, nb)),
            dma((tp, nb)),
            dma((tp, nb)),
            dma((tp, nb)),
        ],
        compiler_params=pltpu.CompilerParams(has_side_effects=True, vmem_limit_bytes=56 << 20),
        name="front",
    )(x, gate, logs, step, taps, hgain, wout, residual, cgain)


def shards(
    grouped_head_inputs,
    head_gate_inputs,
    unsmoothed_step,
    head_decay_rate,
    extra_log_decay,
    first_group_keys,
    first_group_queries,
    second_group_keys,
    second_group_queries,
    head_input_filter,
    first_group_filter,
    second_group_filter,
    head_norm_gain,
    output_weight,
    residual,
    channel_norm_gain,
    channel_gate_weight,
    channel_up_weight,
    channel_down_weight,
):
    tp = lax.axis_size("tp")
    tokens = grouped_head_inputs.shape[0]
    heads = head_decay_rate.shape[1]
    half = heads * HEAD
    s1, s2 = first_group_keys.shape[1], second_group_keys.shape[1]
    gate_full = lax.all_gather(channel_gate_weight, "sp", axis=0, tiled=True)
    up_full = lax.all_gather(channel_up_weight, "sp", axis=0, tiled=True)
    down_full = lax.all_gather(channel_down_weight, "sp", axis=0, tiled=True)
    x = jnp.concatenate(
        [
            grouped_head_inputs.reshape(tokens, 2 * half),
            first_group_keys,
            first_group_queries,
            second_group_keys,
            second_group_queries,
        ],
        axis=1,
    )
    taps = jnp.concatenate(
        [
            head_input_filter.reshape(CONV, 2 * half),
            first_group_filter.reshape(CONV, 2 * s1),
            second_group_filter.reshape(CONV, 2 * s2),
        ],
        axis=1,
    )
    step = jax.nn.softplus(unsmoothed_step.reshape(tokens, 2 * heads))
    logs = extra_log_decay.reshape(tokens, 2 * heads) - step * head_decay_rate.reshape(1, -1)
    pad = ((0, 0), (0, BLOCK - 2 * heads))
    wout = output_weight.reshape(2, tp, half, -1).swapaxes(0, 1).reshape(tp, 2 * half, -1)
    normed, stream = front(
        x,
        head_gate_inputs.reshape(tokens, 2 * half),
        jnp.pad(logs, pad),
        jnp.pad(step, pad),
        taps,
        head_norm_gain.reshape(1, 2 * half),
        wout,
        residual,
        channel_norm_gain.reshape(1, -1),
        heads,
        s1,
        s2,
    )
    gate = jnp.dot(normed, gate_full, preferred_element_type=jnp.float32)
    upward = jnp.dot(normed, up_full, preferred_element_type=jnp.float32)
    hidden = (jax.nn.silu(gate) * upward).astype(jnp.bfloat16)
    partial_value = lax.dot_general(
        hidden, down_full, (((1,), (1,)), ((), ())), preferred_element_type=jnp.float32
    )
    summed = lax.psum_scatter(
        partial_value.astype(jnp.bfloat16), "tp", scatter_dimension=1, tiled=True
    ).astype(jnp.float32)
    return (stream.astype(jnp.float32) + 0.5 * summed).astype(jnp.bfloat16)


def solution(mesh):
    return jax.shard_map(
        shards,
        mesh=mesh,
        in_specs=(
            P("sp", None, "tp"),
            P("sp", None, "tp"),
            P("sp", None, "tp"),
            P(None, "tp"),
            P("sp", None, "tp"),
            P("sp", None),
            P("sp", None),
            P("sp", None),
            P("sp", None),
            P(None, None, "tp"),
            P(),
            P(),
            P(None, "tp"),
            P(None, None, "tp"),
            P("sp", "tp"),
            P(),
            P("sp", "tp"),
            P("sp", "tp"),
            P("sp", "tp"),
        ),
        out_specs=P("sp", "tp"),
        check_vma=False,
    )
```

time: 762 us -> 355 us (0.47)
  local copies, waits for them, and re-layouts: 167 us -> 16.2 us
  waiting for transfers between devices: 356 us -> 219 us
  blocking collectives: 82.6 us -> 0 us
  Pallas kernels: 0 us -> 72.9 us
  matrix products: 79.8 us -> 30 us
  other arithmetic: 36.8 us -> 3.42 us
  starting transfers between devices: 19.6 us -> 0.12 us
    all_gather x5 -> x3, waiting for transfers between devices: 312 us -> 174 us  [the longest x1 87.1 us: shards(): up_full = lax.all_gather(channel_up_weight, 'sp', axis=0, tiled=True)]
    all_gather x3 -> x0, blocking collectives: 82.6 us -> none  [the longest x1 33.7 us: shards(): lax.all_gather(state_one[None].astype(jnp.bfloat16), 'sp', axis=0, tiled=...]
    pallas_call x0 -> x1, Pallas kernels: none -> 72.9 us  [front(): pl.pallas_call(functools.partial(front_kernel, n, tp, heads, s1, s2), out...]
    dynamic_update_slice x16 -> x0, local copies, waits for them, and re-layouts: 71.1 us -> none  [scan_group(): final_state, outputs = lax.scan(advance, initial, blocks)]
    dot_general x70 -> x1, matrix products: 69.1 us -> 19.5 us  [shards(): lax.dot_general(hidden, down_full, (((1,), (1,)), ((), ())), preferred_el...]
    dynamic_slice x24 -> x0, local copies, waits for them, and re-layouts: 30.1 us -> none  [scan_group(): final_state, outputs = lax.scan(advance, initial, blocks)]
    ppermute x5 -> x0, starting transfers between devices: 19.2 us -> none  [from_behind(): return lax.ppermute(block, axis, route)]
    convert_element_type x13 -> x0, other arithmetic: 15.1 us -> none  [the longest x5 7.47 us: causal_taps(): values.astype(jnp.float32)]
  transfers between devices with their start and end apart: 11 -> 4, of which waited for: 6 -> 4; matrix products, arithmetic and copies ran while one was open for 8% -> 8% of each run, Pallas kernels for 0% -> 21%
where the time goes in v1:
time: 355 us; the launch traced here: 354 us
  waiting for transfers between devices  219 us (62%)
  Pallas kernels  72.9 us (21%)
  matrix products  30 us (8%)
  local copies, waits for them, and re-layouts  16.2 us (5%)
  between operations  13.2 us (4%)
    all_gather x1, waiting for transfers between devices, shards(): up_full = lax.all_gather(channel_up_weight, 'sp', axis=0, tiled=True)  87.1 us
    all_gather x1, waiting for transfers between devices, shards(): down_full = lax.all_gather(channel_down_weight, 'sp', axis=0, tiled=True)  86.3 us
    pallas_call x1, Pallas kernels, front(): pl.pallas_call(functools.partial(front_kernel, n, tp, heads, s1, s2), out...  72.9 us
    reduce_scatter x1, waiting for transfers between devices, shards(): lax.psum_scatter(partial_value.astype(jnp.bfloat16), 'tp', scatter_dimens...  42.7 us
    dot_general x1, matrix products, shards(): lax.dot_general(hidden, down_full, (((1,), (1,)), ((), ())), preferred_el...  19.5 us
    dot_general x1, matrix products, shards(): gate = jnp.dot(normed, gate_full, preferred_element_type=jnp.float32)  10.4 us
  transfers between devices with their start and end apart: 4, of which 4 were waited for; matrix products, arithmetic and copies ran while one was open for 8% of the time, Pallas kernels for 21%

profile of v1, /device:TPU:0, one launch (start us, length us, event | category | flops | bytes accessed | tf_op | source)
XLA Modules:
  0.0 354.3 jit_solution(99884062158675135)
XLA Ops:
  6.5 0.7 all-gather.4.cloned.1.call-update
  7.3 0.7 all-gather.6.cloned.1.call-update
  8.1 0.7 all-gather.8.cloned.1.call-update
  8.8 0.8 reshape.38
  9.8 0.8 reshape.37
  10.8 0.8 mul.23
  11.5 0.3 compare_select_fusion
  11.8 0.8 pad.7.log_ref
  12.7 0.8 pad.8.step_ref
  13.5 1.4 copy.47
  15.2 1.8 copy.35
  16.9 1.6 copy.44
  18.5 2.5 copy.48
  21.1 0.6 copy.51
  21.7 3.6 %concatenate.6.x_ref = bf16[1024,896]{1,0:T(8,128)(2,1)} concatenate(bf16[1024,512]{1,0:T(8,128)(2,1)S(1)} %bitcast.29, bf16[1024,128]{1,0:T(8,128)(2,1)} %param.24, bf16[1024,128]{1,0:T(8,128)(2,1)} %param.25, bf16[1024,64]{1,0:T(8,128)(2,1)S(1)} %copy.34, bf16[1024,64]{1,0:T(8,128)(2,1)} %copy.35), dimensions={1} | concatenate | bytes 3670016 | tf_op jit(solution)/shard_map/concatenate | solution.py:374
  25.4 0.6 pad_maximum_fusion.taps_ref
  26.0 72.9 %front.1 = (bf16[1024,2048]{1,0:T(8,128)(2,1)}, bf16[1024,512]{1,0:T(8,128)(2,1)}) custom-call(bf16[1024,896]{1,0:T(8,128)(2,1)} %concatenate.6.x_ref, bf16[1024,512]{1,0:T(8,128)(2,1)} %bitcast.28, f32[1024,128]{1,0:T(8,128)} %pad.7.log_ref, f32[1024,128]{1,0:T(8,128)} %pad.8.step_ref, f32[4,896]{1,0:T(4,128)} %pad_maximum_fusion.taps_ref, ...), custom_call_target="tpu_custom_call" | custom-call | tf_op jit(solution)/shard_map/front/pallas_call | solution.py:311
  98.8 0.3 all-gather.4.cloned.1.call-done
  99.2 10.4 %fusion.1 = f32[1024,1280]{1,0:T(8,128)} fusion(bf16[1024,2048]{1,0:T(8,128)(2,1)} %get-tuple-element.8, bf16[2048,1280]{1,0:T(8,128)(2,1)} %all-gather.4.cloned.1.call-done), kind=kOutput, calls=%fused_computation.8 | convolution fusion | flops 5368709120 | bytes 14680064 | tf_op jit(solution)/shard_map/dot_general | solution.py:410
  109.6 87.1 %all-gather.6.cloned.1.call-done = bf16[2048,1280]{1,0:T(8,128)(2,1)} async-done(((bf16[256,1280]{1,0:T(8,128)(2,1)}), bf16[2048,1280]{1,0:T(8,128)(2,1)}) %all-gather.6.cloned.1.call-update) | async-done | bytes 5242896 | tf_op jit(solution)/shard_map/all_gather | solution.py:372
  196.6 86.3 %all-gather.8.cloned.1.call-done = bf16[2048,1280]{1,0:T(8,128)(2,1)} async-done(((bf16[256,1280]{1,0:T(8,128)(2,1)}), bf16[2048,1280]{1,0:T(8,128)(2,1)}) %all-gather.8.cloned.1.call-update) | async-done | bytes 5242896 | tf_op jit(solution)/shard_map/all_gather | solution.py:373
  282.9 19.5 %convolution_convert_fusion = bf16[1024,2048]{1,0:T(8,128)(2,1)} fusion(bf16[2048,1280]{1,0:T(8,128)(2,1)} %all-gather.8.cloned.1.call-done, f32[1024,1280]{1,0:T(8,128)} %fusion.1, bf16[1024,2048]{1,0:T(8,128)(2,1)} %get-tuple-element.8, bf16[2048,1280]{1,0:T(8,128)(2,1)} %all-gather.6.cloned.1.call-done), kind=kOutput, calls=%fused_computation.1 | convolution fusion | flops 10747379712 | bytes 24117248 | tf_op jit(solution)/shard_map/dot_general | solution.py:413
  302.5 42.7 %reduce-scatter.2.cloned.1.call-done = bf16[1024,512]{1,0:T(8,128)(2,1)} async-done(((bf16[1024,2048]{1,0:T(8,128)(2,1)}), bf16[1024,512]{1,0:T(8,128)(2,1)}) %reduce-scatter.2.cloned.1.call-update) | async-done | bytes 1048592 | tf_op jit(solution)/shard_map/reduce_scatter | solution.py:416
  345.2 2.5 add_convert_fusion
  (25 shorter events, 0.8 us)
Async XLA Ops:
  6.5 8.4 %copy-start.2 = (bf16[1024,64]{0,1:T(8,128)(2,1)S(1)}, bf16[1024,64]{0,1:T(8,128)(2,1)}, u32[]{:S(2)}) copy-start(bf16[1024,64]{0,1:T(8,128)(2,1)} %param.26) | copy-start | bytes 393220
  6.5 10.4 %copy-start = (bf16[2,1024,512]{2,1,0:T(8,128)(2,1)S(1)}, bf16[2,1024,512]{2,1,0:T(8,128)(2,1)}, u32[]{:S(2)}) copy-start(bf16[2,1024,512]{2,1,0:T(8,128)(2,1)} %param.32) | copy-start | bytes 6291460
  6.5 92.6 %all-gather.4.cloned.1.call-start = ((), (), s32[]{:S(2)}) async-start(), calls=%async_computation.1 | async-start | bytes 5898240 | tf_op jit(solution)/shard_map/all_gather | solution.py:371
  7.3 189.4 %all-gather.6.cloned.1.call-start = ((), (), s32[]{:S(2)}) async-start(), calls=%async_computation.2 | async-start | bytes 5898240 | tf_op jit(solution)/shard_map/all_gather | solution.py:372
  8.0 274.9 %all-gather.8.cloned.1.call-start = ((), (), s32[]{:S(2)}) async-start(), calls=%async_computation.3 | async-start | bytes 5898240 | tf_op jit(solution)/shard_map/all_gather | solution.py:373
  8.7 336.5 %reduce-scatter.2.cloned.1.call-start = ((), (), s32[]{:S(2)}) async-start(), calls=%async_computation.4 | async-start | bytes 5242880 | tf_op jit(solution)/shard_map/reduce_scatter | solution.py:416
  12.7 8.3 %copy-start.3 = (f32[4,2,256]{2,1,0:T(2,128)S(1)}, f32[4,2,256]{2,1,0:T(2,128)}, u32[]{:S(2)}) copy-start(f32[4,2,256]{2,1,0:T(2,128)} %param.28) | copy-start | bytes 24580
  12.7 8.3 %copy-start.5 = (f32[4,2,128]{2,1,0:T(2,128)S(1)}, f32[4,2,128]{2,1,0:T(2,128)}, u32[]{:S(2)}) copy-start(f32[4,2,128]{2,1,0:T(2,128)} %param.29) | copy-start | bytes 12292
  12.7 8.4 %copy-start.4 = (f32[4,2,64]{2,1,0:T(2,128)S(1)}, f32[4,2,64]{2,1,0:T(2,128)}, u32[]{:S(2)}) copy-start(f32[4,2,64]{2,1,0:T(2,128)} %param.30) | copy-start | bytes 6148
  15.2 6.0 %copy-start.6 = (f32[2,256]{1,0:T(2,128)S(1)}, f32[2,256]{1,0:T(2,128)}, u32[]{:S(2)}) copy-start(f32[2,256]{1,0:T(2,128)} %param.31) | copy-start | bytes 6148
  109.6 235.6 %copy-start.1 = (bf16[1024,512]{1,0:T(8,128)(2,1)S(1)}, bf16[1024,512]{1,0:T(8,128)(2,1)}, u32[]{:S(2)}) copy-start(bf16[1024,512]{1,0:T(8,128)(2,1)} %get-tuple-element.7) | copy-start | bytes 3145732
Sparse Core Ops, SparseCore 0:
  9.5 89.6 all-gather.3
  101.3 95.2 all-gather.5
  198.8 84.0 all-gather.7
  302.6 42.5 reduce-scatter.1
